TPU v7x, 32 devices: a whole 2x2x4 slice. The times are simulated.
32 devices in a mesh: sp: 16 (over z, y, x), tp: 2 (over core).
Axes of the slice: x: 2, y: 2, z: 4, core: 2. Of those that a mesh axis runs over, the one named last changes fastest.
Arguments:
- resid: bfloat16 [3072, 2048], P(('sp', 'tp')), may hold values from -6 to 6
- queries: bfloat16 [3072, 2048], P('sp', 'tp'), may hold values from -8 to 8
- keys: bfloat16 [3072, 512], P('sp', 'tp'), may hold values from -8 to 8
- values: bfloat16 [3072, 512], P('sp', 'tp'), may hold values from -6 to 6
- log_gates: float32 [3072, 32], P('sp', 'tp'), may hold values from -1536 to 0, as said below
- out_gate: bfloat16 [3072, 2048], P('sp', 'tp'), may hold values from -8 to 8
- out_weight: bfloat16 [2048, 2048], P('tp'), may hold values from -0.125 to 0.125
- post_gain: float32 [2048], replicated, may hold values from 0.1 to 1.9
- pre_gain: float32 [2048], replicated, may hold values from 0.1 to 1.9
- ffn_gain: float32 [2048], replicated, may hold values from 0.1 to 1.9
- gate_weight: bfloat16 [2048, 5632], P('sp', 'tp'), may hold values from -0.125 to 0.125
- up_weight: bfloat16 [2048, 5632], P('sp', 'tp'), may hold values from -0.125 to 0.125
- down_weight: bfloat16 [5632, 2048], P('tp', 'sp'), may hold values from -0.078125 to 0.078125
Outputs:
- result: bfloat16 [3072, 2048], P(('sp', 'tp'))
Inputs may be any that keep to these rules, and one draw needn't show every extreme that they name: Each head's column of log_gates never rises from one position to the next, and its first entry is at most 0.
All inputs are finite; a program needn't handle non-finite values.
Results may differ from a plain program's by a relative error of at most 0.017.
Values may be sent and summed in bfloat16 or wider, within the bound.
A program may use at most 128 MiB of HBM per device.

v0:
```python
import jax
import jax.numpy as jnp
from jax import lax
from jax.sharding import PartitionSpec as P

HD = 64
EPS = 1e-06
KEY_BLOCK = 512


def rms_scale(rows, gain):
    mean_sq = jnp.mean(rows * rows, axis=-1, keepdims=True)
    return rows * lax.rsqrt(mean_sq + EPS) * gain


def shards(
    resid,
    queries,
    keys,
    values,
    log_gates,
    out_gate,
    out_weight,
    post_gain,
    pre_gain,
    ffn_gain,
    gate_weight,
    up_weight,
    down_weight,
):
    rows = queries.shape[0]
    head_size = HD
    kv_local = keys.shape[1] // head_size
    q_local = queries.shape[1] // head_size
    group = q_local // kv_local
    scale = head_size ** (-0.5)
    offset = lax.axis_index("sp") * rows
    last = offset + rows - 1
    query_pos = offset + jnp.arange(rows, dtype=jnp.int32)
    key_gates = lax.all_gather(log_gates, "sp", axis=0, tiled=True)
    query_blocks = queries.reshape(rows, kv_local, group, head_size)
    query_gates = log_gates.reshape(rows, kv_local, group).transpose(1, 2, 0)

    def key_block(carry, key_rows, value_rows, start):
        count = key_rows.shape[0]

        def compute(state):
            top, denom, accum = state
            scores = (
                jnp.einsum(
                    "tkgd,skd->kgts",
                    query_blocks,
                    key_rows.reshape(count, kv_local, head_size),
                    preferred_element_type=jnp.float32,
                )
                * scale
            )
            gates_here = (
                lax.dynamic_slice_in_dim(key_gates, start, count, 0)
                .reshape(count, kv_local, group)
                .transpose(1, 2, 0)
            )
            scores = scores + query_gates[:, :, :, None] - gates_here[:, :, None, :]
            causal = (start + jnp.arange(count, dtype=jnp.int32))[None, :] <= query_pos[:, None]
            scores = jnp.where(causal[None, None], scores, -jnp.inf)
            new_top = jnp.maximum(top, jnp.max(scores, axis=-1))
            shrink = jnp.exp(top - new_top)
            weights = jnp.exp(scores - new_top[..., None])
            denom = denom * shrink + jnp.sum(weights, axis=-1)
            accum = accum * shrink[..., None] + jnp.einsum(
                "kgts,skd->kgtd",
                weights.astype(jnp.bfloat16),
                value_rows.reshape(count, kv_local, head_size),
                preferred_element_type=jnp.float32,
            )
            return (new_top, denom, accum)

        def keep(state):
            return state

        return lax.cond(start <= last, compute, keep, carry)

    start_state = (
        jnp.full((kv_local, group, rows), -1e30, jnp.float32),
        jnp.zeros((kv_local, group, rows), jnp.float32),
        jnp.zeros((kv_local, group, rows, head_size), jnp.float32),
    )
    carry = start_state
    key_rows = lax.all_gather(keys, "sp", axis=0, tiled=True)
    value_rows = lax.all_gather(values, "sp", axis=0, tiled=True)
    count = key_rows.shape[0]
    blocks = count // KEY_BLOCK
    key_split = key_rows.reshape(blocks, KEY_BLOCK, key_rows.shape[1])
    value_split = value_rows.reshape(blocks, KEY_BLOCK, value_rows.shape[1])

    def advance(state, item):
        index, key_part, value_part = item
        return (key_block(state, key_part, value_part, index * KEY_BLOCK), None)

    carry, _ = lax.scan(
        advance, carry, (jnp.arange(blocks, dtype=jnp.int32), key_split, value_split)
    )
    top, denom, accum = carry
    attended = (accum / denom[..., None]).transpose(2, 0, 1, 3).reshape(rows, q_local * head_size)
    gated = (attended * jax.nn.sigmoid(out_gate.astype(jnp.float32))).astype(jnp.bfloat16)
    projected = lax.psum_scatter(
        jnp.dot(gated, out_weight, preferred_element_type=jnp.float32).astype(jnp.bfloat16),
        "tp",
        scatter_dimension=0,
        tiled=True,
    ).astype(jnp.float32)
    mixed = resid.astype(jnp.float32) + rms_scale(projected, post_gain)
    normed = rms_scale(mixed, pre_gain).astype(jnp.bfloat16)
    normed_all = lax.all_gather(normed, "tp", axis=0, tiled=True)
    gate = jnp.dot(
        normed_all,
        lax.all_gather(gate_weight, "sp", axis=0, tiled=True),
        preferred_element_type=jnp.float32,
    )
    up = jnp.dot(
        normed_all,
        lax.all_gather(up_weight, "sp", axis=0, tiled=True),
        preferred_element_type=jnp.float32,
    )
    hidden = (jax.nn.silu(gate) * up).astype(jnp.bfloat16)
    ffn_partial = jnp.dot(
        hidden,
        lax.all_gather(down_weight, "sp", axis=1, tiled=True),
        preferred_element_type=jnp.float32,
    )
    ffn = lax.psum_scatter(
        ffn_partial.astype(jnp.bfloat16), "tp", scatter_dimension=0, tiled=True
    ).astype(jnp.float32)
    return (mixed + rms_scale(ffn, ffn_gain)).astype(jnp.bfloat16)


def solution(mesh):
    in_specs = (
        P(("sp", "tp"), None),
        P("sp", "tp"),
        P("sp", "tp"),
        P("sp", "tp"),
        P("sp", "tp"),
        P("sp", "tp"),
        P("tp", None),
        P(),
        P(),
        P(),
        P("sp", "tp"),
        P("sp", "tp"),
        P("tp", "sp"),
    )
    out_specs = P(("sp", "tp"), None)
    return jax.shard_map(shards, mesh=mesh, in_specs=in_specs, out_specs=out_specs, check_vma=False)
```

profile of v0, /device:TPU:0, one launch (start us, length us, event | category | flops | bytes accessed | tf_op | source)
XLA Modules:
  0.0 712.2 jit_solution(13522817512439941888)
XLA Ops:
  6.5 0.7 all-gather.7.cloned.1.call-update
  7.3 0.7 all-gather.9.cloned.1.call-update
  8.0 0.0 reduce-scatter.3.cloned.1.call-start
  8.1 0.7 reshape.101
  8.8 44.2 %all-gather = f32[16,192,16]{1,2,0:T(8,128)S(1)} all-gather(f32[1,192,16]{1,2,0:T(8,128)} %bitcast.74), channel_id=1, replica_groups=mesh['sp'=16,'tp'=2] {'sp'}, dimensions={0}, use_global_device_ids=true | all-gather | bytes 208896 | tf_op jit(solution)/shard_map/all_gather | solution.py:40
  52.9 0.2 copy.27
  53.1 0.1 reshape.105
  53.2 2.0 copy.26
  55.2 15.7 %all-gather.7.cloned.1.call-done = bf16[3072,256]{1,0:T(8,128)(2,1)} async-done(((bf16[192,256]{1,0:T(8,128)(2,1)}), bf16[3072,256]{1,0:T(8,128)(2,1)}) %all-gather.7.cloned.1.call-update) | async-done | bytes 1572880 | tf_op jit(solution)/shard_map/all_gather | solution.py:89
  70.9 1.7 copy.28
  72.7 57.8 %all-gather.9.cloned.1.call-done = bf16[3072,256]{1,0:T(8,128)(2,1)} async-done(((bf16[192,256]{1,0:T(8,128)(2,1)}), bf16[3072,256]{1,0:T(8,128)(2,1)}) %all-gather.9.cloned.1.call-update) | async-done | bytes 1572880 | tf_op jit(solution)/shard_map/all_gather | solution.py:90
  130.4 1.7 copy.29
  132.2 1.1 broadcast_in_dim.42
  133.3 17.4 %while.15 = (s32[]{:T(128)}, f32[4,4,192]{2,1,0:T(4,128)S(1)}, f32[4,4,192]{2,1,0:T(4,128)S(1)}, f32[4,4,192,64]{2,3,1,0:T(8,128)}, s32[6]{0:T(128)S(1)}, /*inde...) while((s32[]{:T(128)}, f32[4,4,192]{2,1,0:T(4,128)S(1)}, ...), condition=%wide.region_5.6_spmd.clone, body=%wide.region_0.5_spmd.clone.sunk | while | flops 429890240 | bytes 29568428 | solution.py:100
  133.3 0.6 dynamic_slice.31
  134.5 9.6 %conditional.3 = ((f32[4,4,192]{2,1,0:T(4,128)S(1)}, f32[4,4,192]{2,1,0:T(4,128)S(1)}, f32[4,4,192,64]{2,3,1,0:T(8,128)})) conditional(s32[]{:T(128)} %convert_element_type.96, (f32[4,4,192]{2,1,0:T(4,128)S(1)}, f32[4,4,192]{2,1,0:T(4,128)S(1)}, f32[4,4,192,64]{2,3,1,0:T(8,128)}) %tuple.43, (s32[]{:T(128)}, s32[]{:T(128)}, ...), branch_computations={%region_1.1_spmd, %region_2.4_spmd} | conditional | flops 429890240 | bytes 29567370 | solution.py:81
  134.5 0.1 constant_dynamic-slice_fusion.1
  134.7 0.1 broadcast_compare_fusion
  134.9 3.4 fusion.6
  138.2 2.5 fusion.5
  140.8 2.3 fusion.10
  143.1 1.0 copy-done.2
  144.1 0.6 dynamic_slice.31
  145.4 0.6 dynamic_slice.31
  146.7 0.6 dynamic_slice.31
  148.0 0.6 dynamic_slice.31
  149.3 0.6 dynamic_slice.31
  150.6 1.3 broadcast_divide_fusion
  152.0 0.3 copy.30
  152.3 4.3 convolution_convert_fusion.1
  156.6 0.0 all-gather.11.cloned.1.call-start
  156.7 0.5 all-gather.11.cloned.1.call-update
  157.3 0.5 all-gather.13.cloned.1.call-update
  157.8 0.5 all-gather.15.cloned.1.call-update
  158.4 0.0 reduce-scatter.5.cloned.1.call-start
  158.4 53.0 %reduce-scatter.3.cloned.1.call-done = bf16[96,2048]{1,0:T(8,128)(2,1)} async-done(((bf16[192,2048]{1,0:T(8,128)(2,1)}), bf16[96,2048]{1,0:T(8,128)(2,1)}) %reduce-scatter.3.cloned.1.call-update) | async-done | bytes 393232 | tf_op jit(solution)/shard_map/reduce_scatter | solution.py:106
  211.4 1.2 fusion.16
  212.6 1.3 multiply_reduce_fusion
  214.0 1.3 multiply_convert_fusion
  215.3 2.5 all_gather.24
  217.8 138.8 %all-gather.11.cloned.1.call-done = bf16[2048,2816]{1,0:T(8,128)(2,1)} async-done(((bf16[128,2816]{1,0:T(8,128)(2,1)}), bf16[2048,2816]{1,0:T(8,128)(2,1)}) %all-gather.11.cloned.1.call-update) | async-done | bytes 11534352 | tf_op jit(solution)/shard_map/all_gather | solution.py:117
  356.6 8.0 %fusion.26 = f32[192,2816]{1,0:T(8,128)} fusion(bf16[192,2048]{1,0:T(8,128)(2,1)S(1)} %all_gather.24, bf16[2048,2816]{1,0:T(8,128)(2,1)} %all-gather.11.cloned.1.call-done), kind=kOutput, calls=%fused_computation.46 | convolution fusion | flops 2214592512 | bytes 14483456 | tf_op jit(solution)/shard_map/dot_general | solution.py:115
  364.6 134.2 %all-gather.13.cloned.1.call-done = bf16[2048,2816]{1,0:T(8,128)(2,1)} async-done(((bf16[128,2816]{1,0:T(8,128)(2,1)}), bf16[2048,2816]{1,0:T(8,128)(2,1)}) %all-gather.13.cloned.1.call-update) | async-done | bytes 11534352 | tf_op jit(solution)/shard_map/all_gather | solution.py:122
  498.8 182.8 %all-gather.15.cloned.1.call-done = bf16[2816,2048]{1,0:T(8,128)(2,1)} async-done(((bf16[2816,128]{1,0:T(8,128)(2,1)}), bf16[2816,2048]{1,0:T(8,128)(2,1)}) %all-gather.15.cloned.1.call-update) | async-done | bytes 11534352 | tf_op jit(solution)/shard_map/all_gather | solution.py:128
  681.6 13.9 %convolution_convert_fusion = bf16[192,2048]{1,0:T(8,128)(2,1)} fusion(bf16[2816,2048]{1,0:T(8,128)(2,1)} %all-gather.15.cloned.1.call-done, bf16[192,2048]{1,0:T(8,128)(2,1)S(1)} %all_gather.24, bf16[2048,2816]{1,0:T(8,128)(2,1)} %all-gather.13.cloned.1.call-done, f32[192,2816]{1,0:T(8,128)} %fusion.26), kind=kOutput, calls=%fused_computation.23 | convolution fusion | flops 4432822272 | bytes 26804224 | tf_op jit(solution)/shard_map/dot_general | solution.py:126
  695.5 6.5 reduce-scatter.5.cloned.1.call-done
  702.0 1.2 fusion.19
  703.2 2.1 fusion.22
  (43 shorter events, 0.4 us)
Async XLA Ops:
  6.5 64.4 %all-gather.7.cloned.1.call-start = ((), (), s32[]{:S(2)}) async-start(), calls=%async_computation.2 | async-start | bytes 1671168 | tf_op jit(solution)/shard_map/all_gather | solution.py:89
  7.3 123.2 %all-gather.9.cloned.1.call-start = ((), (), s32[]{:S(2)}) async-start(), calls=%async_computation.3 | async-start | bytes 1671168 | tf_op jit(solution)/shard_map/all_gather | solution.py:90
  8.0 203.4 %reduce-scatter.3.cloned.1.call-start = ((), (), s32[]{:S(2)}) async-start(), calls=%async_computation.4 | async-start | bytes 1179648 | tf_op jit(solution)/shard_map/reduce_scatter | solution.py:106
  134.8 6.0 copy-start.1
  143.1 1.0 copy-start.2
  152.3 60.3 %copy-start.3 = (bf16[96,2048]{1,0:T(8,128)(2,1)S(1)}, bf16[96,2048]{1,0:T(8,128)(2,1)}, u32[]{:S(2)}) copy-start(bf16[96,2048]{1,0:T(8,128)(2,1)} %param.17) | copy-start | bytes 1179652
  152.3 60.3 %copy-start.4 = (f32[2048]{0:T(1024)S(1)}, f32[2048]{0:T(1024)}, u32[]{:S(2)}) copy-start(f32[2048]{0:T(1024)} %param.24) | copy-start | bytes 24580
  152.3 61.7 %copy-start.5 = (f32[2048]{0:T(1024)S(1)}, f32[2048]{0:T(1024)}, u32[]{:S(2)}) copy-start(f32[2048]{0:T(1024)} %param.25) | copy-start | bytes 24580
  156.6 200.0 %all-gather.11.cloned.1.call-start = ((), (), s32[]{:S(2)}) async-start(), calls=%async_computation.5 | async-start | bytes 12255232 | tf_op jit(solution)/shard_map/all_gather | solution.py:117
  157.2 341.6 %all-gather.13.cloned.1.call-start = ((), (), s32[]{:S(2)}) async-start(), calls=%async_computation.6 | async-start | bytes 12255232 | tf_op jit(solution)/shard_map/all_gather | solution.py:122
  157.8 523.8 %all-gather.15.cloned.1.call-start = ((), (), s32[]{:S(2)}) async-start(), calls=%async_computation.7 | async-start | bytes 12255232 | tf_op jit(solution)/shard_map/all_gather | solution.py:128
  158.4 543.6 %reduce-scatter.5.cloned.1.call-start = ((), (), s32[]{:S(2)}) async-start(), calls=%async_computation.8 | async-start | bytes 1179648 | tf_op jit(solution)/shard_map/reduce_scatter | solution.py:131
  364.6 338.6 %copy-start = (bf16[96,2048]{1,0:T(8,128)(2,1)S(1)}, bf16[96,2048]{1,0:T(8,128)(2,1)}, u32[]{:S(2)}) copy-start(bf16[96,2048]{1,0:T(8,128)(2,1)} %reduce-scatter.3.cloned.1.call-done) | copy-start | bytes 1179652
  364.6 338.6 %copy-start.6 = (f32[2048]{0:T(1024)S(1)}, f32[2048]{0:T(1024)}, u32[]{:S(2)}) copy-start(f32[2048]{0:T(1024)} %param.26) | copy-start | bytes 24580
Sparse Core Ops, SparseCore 0:
  10.1 60.7 all-gather.6
  73.7 56.6 all-gather.8
  156.8 54.6 reduce-scatter.2
  214.0 142.5 all-gather.10
  359.2 139.5 all-gather.12
  501.4 180.2 all-gather.14
  695.6 6.3 reduce-scatter.4
where the time goes:
time: 713 us; the launch traced here: 712 us
  waiting for transfers between devices  592 us (83%)
  blocking collectives  46.7 us (7%)
  matrix products  31.8 us (4%)
  between operations  13.6 us (2%)
  local copies, waits for them, and re-layouts  12.7 us (2%)
  other arithmetic  11.1 us (2%)
    all_gather x1, waiting for transfers between devices, shards(): lax.all_gather(down_weight, 'sp', axis=1, tiled=True)  183 us
    all_gather x1, waiting for transfers between devices, shards(): lax.all_gather(gate_weight, 'sp', axis=0, tiled=True)  139 us
    all_gather x1, waiting for transfers between devices, shards(): lax.all_gather(up_weight, 'sp', axis=0, tiled=True)  134 us
    all_gather x1, waiting for transfers between devices, shards(): value_rows = lax.all_gather(values, 'sp', axis=0, tiled=True)  57.8 us
    reduce_scatter x1, waiting for transfers between devices, shards(): lax.psum_scatter(jnp.dot(gated, out_weight, preferred_element_type=jnp.fl...  53 us
    all_gather x1, blocking collectives, shards(): key_gates = lax.all_gather(log_gates, 'sp', axis=0, tiled=True)  44.2 us
    all_gather x1, waiting for transfers between devices, shards(): key_rows = lax.all_gather(keys, 'sp', axis=0, tiled=True)  15.7 us
  transfers between devices with their start and end apart: 7, of which 7 were waited for; matrix products, arithmetic and copies ran while one was open for 2% of the time, Pallas kernels for 0%

commit v1 on v0

--- a/solution.py
+++ b/solution.py
@@ -6,6 +6,18 @@
 HD = 64
 EPS = 1e-06
 KEY_BLOCK = 512
+
+
+def gather_by_bits(x, axis, dim):
+    ways, here, step = (lax.axis_size(axis), lax.axis_index(axis), x.shape[dim])
+    line, have = (x, 1)
+    while have < ways:
+        line = jnp.concatenate(
+            [line, lax.ppermute(line, axis, [(d, (d - have) % ways) for d in range(ways)])],
+            axis=dim,
+        )
+        have = 2 * have
+    return jnp.roll(line, here * step, axis=dim)
 
 
 def rms_scale(rows, gain):
@@ -124,9 +136,7 @@
     )
     hidden = (jax.nn.silu(gate) * up).astype(jnp.bfloat16)
     ffn_partial = jnp.dot(
-        hidden,
-        lax.all_gather(down_weight, "sp", axis=1, tiled=True),
-        preferred_element_type=jnp.float32,
+        hidden, gather_by_bits(down_weight, "sp", 1), preferred_element_type=jnp.float32
     )
     ffn = lax.psum_scatter(
         ffn_partial.astype(jnp.bfloat16), "tp", scatter_dimension=0, tiled=True

time: 713 us -> 843 us (1.18)
  starting transfers between devices: 0.23 us -> 53.2 us
  waiting for transfers between devices: 592 us -> 637 us
  local copies, waits for them, and re-layouts: 12.7 us -> 39 us
    ppermute x0 -> x4, waiting for transfers between devices: none -> 460 us  [gather_by_bits(): lax.ppermute(line, axis, [(d, (d - have) % ways) for d in range(ways)])]
    all_gather x1 -> x0, waiting for transfers between devices: 183 us -> none  [shards(): lax.all_gather(down_weight, 'sp', axis=1, tiled=True)]
    all_gather x1, waiting for transfers between devices: 139 us -> 0.01 us  [shards(): lax.all_gather(gate_weight, 'sp', axis=0, tiled=True)]
    reduce_scatter x1, waiting for transfers between devices: 53 us -> 0.01 us  [shards(): lax.psum_scatter(jnp.dot(gated, out_weight, preferred_element_type=jnp.fl...]
    ppermute x0 -> x4, starting transfers between devices: none -> 53 us  [gather_by_bits(): lax.ppermute(line, axis, [(d, (d - have) % ways) for d in range(ways)])]
    all_gather x1, waiting for transfers between devices: 134 us -> 94.9 us  [shards(): lax.all_gather(up_weight, 'sp', axis=0, tiled=True)]
    unnamed x14 -> x37, local copies, waits for them, and re-layouts: 5.59 us -> 25.2 us
  transfers between devices with their start and end apart: 7 -> 10, of which waited for: 7 -> 8; matrix products, arithmetic and copies ran while one was open for 2% -> 6% of each run, Pallas kernels for 0% -> 0%
where the time goes in v1:
time: 843 us; the launch traced here: 842 us
  waiting for transfers between devices  637 us (76%)
  starting transfers between devices  53.2 us (6%)
  blocking collectives  47.4 us (6%)
  local copies, waits for them, and re-layouts  39 us (5%)
  matrix products  31.9 us (4%)
  other arithmetic  15.6 us (2%)
  between operations  13.7 us (2%)
    ppermute x4, waiting for transfers between devices, gather_by_bits(): lax.ppermute(line, axis, [(d, (d - have) % ways) for d in range(ways)])  460 us
    all_gather x1, waiting for transfers between devices, shards(): lax.all_gather(up_weight, 'sp', axis=0, tiled=True)  94.9 us
    all_gather x1, waiting for transfers between devices, shards(): value_rows = lax.all_gather(values, 'sp', axis=0, tiled=True)  57.8 us
    ppermute x4, starting transfers between devices, gather_by_bits(): lax.ppermute(line, axis, [(d, (d - have) % ways) for d in range(ways)])  53 us
    all_gather x1, blocking collectives, shards(): key_gates = lax.all_gather(log_gates, 'sp', axis=0, tiled=True)  44.7 us
    unnamed x37, local copies, waits for them, and re-layouts  25.2 us
  transfers between devices with their start and end apart: 10, of which 8 were waited for; matrix products, arithmetic and copies ran while one was open for 6% of the time, Pallas kernels for 0%

profile of v1, /device:TPU:0, one launch (start us, length us, event | category | flops | bytes accessed | tf_op | source)
XLA Modules:
  0.0 842.0 jit_solution(17524650583719050473)
XLA Ops:
  6.5 0.7 all-gather.6.cloned.1.call-update
  7.3 0.7 all-gather.8.cloned.1.call-update
  8.1 2.0 copy.26
  10.1 0.7 reshape.101
  10.8 44.7 %all-gather = f32[16,192,16]{1,2,0:T(8,128)S(1)} all-gather(f32[1,192,16]{1,2,0:T(8,128)} %bitcast.73), channel_id=1, replica_groups=mesh['sp'=16,'tp'=2] {'sp'}, dimensions={0}, use_global_device_ids=true | all-gather | bytes 208896 | tf_op jit(solution)/shard_map/all_gather | solution.py:52
  55.8 15.2 %all-gather.6.cloned.1.call-done = bf16[3072,256]{1,0:T(8,128)(2,1)} async-done(((bf16[192,256]{1,0:T(8,128)(2,1)}), bf16[3072,256]{1,0:T(8,128)(2,1)}) %all-gather.6.cloned.1.call-update) | async-done | bytes 1572880 | tf_op jit(solution)/shard_map/all_gather | solution.py:101
  71.0 1.7 copy.28
  72.7 57.8 %all-gather.8.cloned.1.call-done = bf16[3072,256]{1,0:T(8,128)(2,1)} async-done(((bf16[192,256]{1,0:T(8,128)(2,1)}), bf16[3072,256]{1,0:T(8,128)(2,1)}) %all-gather.8.cloned.1.call-update) | async-done | bytes 1572880 | tf_op jit(solution)/shard_map/all_gather | solution.py:102
  130.5 1.7 copy.29
  132.2 1.1 broadcast_in_dim.42
  133.3 17.7 %while.15 = (s32[]{:T(128)}, f32[4,4,192]{2,1,0:T(4,128)S(1)}, f32[4,4,192]{2,1,0:T(4,128)S(1)}, f32[4,4,192,64]{2,3,1,0:T(8,128)}, s32[6]{0:T(128)S(1)}, /*inde...) while((s32[]{:T(128)}, f32[4,4,192]{2,1,0:T(4,128)S(1)}, ...), condition=%wide.region_5.6_spmd.clone, body=%wide.region_0.5_spmd.clone.sunk | while | flops 429890240 | bytes 29568436 | solution.py:112
  134.6 9.6 %conditional.3 = ((f32[4,4,192]{2,1,0:T(4,128)S(1)}, f32[4,4,192]{2,1,0:T(4,128)S(1)}, f32[4,4,192,64]{2,3,1,0:T(8,128)})) conditional(s32[]{:T(128)} %convert_element_type.96, (f32[4,4,192]{2,1,0:T(4,128)S(1)}, f32[4,4,192]{2,1,0:T(4,128)S(1)}, f32[4,4,192,64]{2,3,1,0:T(8,128)}) %tuple.43, (s32[]{:T(128)}, s32[]{:T(128)}, ...), branch_computations={%region_1.1_spmd, %region_2.4_spmd} | conditional | flops 429890240 | bytes 29567370 | solution.py:93
  135.0 3.4 fusion.6
  138.4 2.5 fusion.5
  140.9 2.3 fusion.10
  143.3 1.0 copy-done.8
  145.6 0.7 dynamic_slice.40
  147.0 0.7 dynamic_slice.40
  149.6 0.7 dynamic_slice.40
  151.0 1.3 broadcast_divide_fusion
  152.7 4.2 convolution_convert_fusion
  158.1 50.9 %collective-permute-start = (bf16[2816,128]{1,0:T(8,128)(2,1)S(1)}, bf16[2816,128]{1,0:T(8,128)(2,1)S(1)}, u32[]{:S(2)}, u32[]{:S(2)}) collective-permute-start(bf16[2816,128]{1,0:T(8,128)(2,1)S(1)} %copy-done.2), channel_id=1, source_target_pairs={{0,30},{2,0},{4,2},{6,4},{8,6},{10,8},{12,10},{14,12},{16,14},{18,... | collective-permute-start | bytes 2162696 | tf_op jit(solution)/shard_map/ppermute | solution.py:16
  209.0 14.0 %collective-permute-done = bf16[2816,128]{1,0:T(8,128)(2,1)S(1)} collective-permute-done((bf16[2816,128]{1,0:T(8,128)(2,1)S(1)}, bf16[2816,128]{1,0:T(8,128)(2,1)S(1)}, u32[]{:S(2)}, u32[]{:S(2)}) %collective-permute-start) | collective-permute-done | bytes 720928 | tf_op jit(solution)/shard_map/ppermute | solution.py:16
  223.2 1.9 collective-permute-start.1
  225.1 45.9 %collective-permute-done.1 = bf16[2816,256]{1,0:T(8,128)(2,1)S(1)} collective-permute-done((bf16[2816,256]{1,0:T(8,128)(2,1)S(1)}, bf16[2816,256]{1,0:T(8,128)(2,1)S(1)}, u32[]{:S(2)}, u32[]{:S(2)}) %collective-permute-start.1) | collective-permute-done | bytes 1441824 | tf_op jit(solution)/shard_map/ppermute | solution.py:16
  271.3 59.4 %collective-permute-done.2 = bf16[2816,512]{1,0:T(8,128)(2,1)S(1)} collective-permute-done((bf16[2816,512]{1,0:T(8,128)(2,1)S(1)}, bf16[2816,512]{1,0:T(8,128)(2,1)S(1)}, u32[]{:S(2)}, u32[]{:S(2)}) %collective-permute-start.2) | collective-permute-done | bytes 2883616 | tf_op jit(solution)/shard_map/ppermute | solution.py:16
  330.8 4.1 pad_maximum_fusion
  335.0 2.1 constant_dynamic-update-slice_fusion.9
  337.1 2.1 constant_dynamic-update-slice_fusion.8
  339.1 2.8 constant_dynamic-update-slice_fusion.7
  342.0 1.2 fusion.21
  343.2 1.3 multiply_reduce_fusion
  344.6 1.3 multiply_convert_fusion
  345.8 2.7 all_gather.21
  348.5 1.9 constant_dynamic-update-slice_fusion.6
  350.4 340.8 %collective-permute-done.3 = bf16[2816,1024]{1,0:T(8,128)(2,1)} collective-permute-done((bf16[2816,1024]{1,0:T(8,128)(2,1)}, bf16[2816,1024]{1,0:T(8,128)(2,1)}, u32[]{:S(2)}, u32[]{:S(2)}) %collective-permute-start.3) | collective-permute-done | bytes 5767200 | tf_op jit(solution)/shard_map/ppermute | solution.py:16
  691.2 5.7 constant_dynamic-update-slice_fusion.5
  696.9 0.9 constant_dynamic-update-slice_fusion.4
  697.9 1.0 constant_dynamic-update-slice_fusion.3
  698.8 1.2 constant_dynamic-update-slice_fusion.2
  700.1 1.8 constant_dynamic-update-slice_fusion.1
  701.9 6.4 constant_dynamic-update-slice_fusion
  708.3 8.1 fusion.32
  716.4 94.9 %all-gather.12.cloned.1.call-done = bf16[2048,2816]{1,0:T(8,128)(2,1)} async-done(((bf16[128,2816]{1,0:T(8,128)(2,1)}), bf16[2048,2816]{1,0:T(8,128)(2,1)}) %all-gather.12.cloned.1.call-update) | async-done | bytes 11534352 | tf_op jit(solution)/shard_map/all_gather | solution.py:134
  811.3 13.9 %fusion.18 = bf16[192,2048]{1,0:T(8,128)(2,1)} fusion(bf16[2816,4096]{1,0:T(8,128)(2,1)} %constant_dynamic-update-slice_fusion, s32[]{:T(128)S(6)} %select_n.25, bf16[192,2048]{1,0:T(8,128)(2,1)S(1)} %copy-done.10, bf16[2048,2816]{1,0:T(8,128)(2,1)} %all-gather.12.cloned.1.call-done, f32[192,2816]{1,0:T(8,128)} %fusion.32), kind=kOutput, calls=%fused_computation.27 | convolution fusion | flops 4432822272 | bytes 26804228 | tf_op jit(solution)/shard_map/dot_general | solution.py:138
  825.2 6.6 reduce-scatter.5.cloned.1.call-done
  831.8 1.2 fusion.24
  833.0 2.1 fusion.27
  (75 shorter events, 4.8 us)
Async XLA Ops:
  6.5 64.5 %all-gather.6.cloned.1.call-start = ((), (), s32[]{:S(2)}) async-start(), calls=%async_computation.2 | async-start | bytes 1671168 | tf_op jit(solution)/shard_map/all_gather | solution.py:101
  7.3 123.2 %all-gather.8.cloned.1.call-start = ((), (), s32[]{:S(2)}) async-start(), calls=%async_computation.3 | async-start | bytes 1671168 | tf_op jit(solution)/shard_map/all_gather | solution.py:102
  8.0 334.0 %reduce-scatter.3.cloned.1.call-start = ((), (), s32[]{:S(2)}) async-start(), calls=%async_computation.4 | async-start | bytes 1179648 | tf_op jit(solution)/shard_map/reduce_scatter | solution.py:118
  135.0 6.0 copy-start.7
  143.3 1.0 copy-start.8
  152.3 5.8 copy-start.2
  156.9 551.4 %all-gather.10.cloned.1.call-start = ((), (), s32[]{:S(2)}) async-start(), calls=%async_computation.5 | async-start | bytes 12255232 | tf_op jit(solution)/shard_map/all_gather | solution.py:129
  157.5 653.8 %all-gather.12.cloned.1.call-start = ((), (), s32[]{:S(2)}) async-start(), calls=%async_computation.6 | async-start | bytes 12255232 | tf_op jit(solution)/shard_map/all_gather | solution.py:134
  158.1 673.7 %reduce-scatter.5.cloned.1.call-start = ((), (), s32[]{:S(2)}) async-start(), calls=%async_computation.7 | async-start | bytes 1179648 | tf_op jit(solution)/shard_map/reduce_scatter | solution.py:141
  158.1 64.9 %collective-permute-start = (bf16[2816,128]{1,0:T(8,128)(2,1)S(1)}, bf16[2816,128]{1,0:T(8,128)(2,1)S(1)}, u32[]{:S(2)}, u32[]{:S(2)}) collective-permute-start(bf16[2816,128]{1,0:T(8,128)(2,1)S(1)} %copy-done.2), channel_id=1, source_target_pairs={{0,30},{2,0},{4,2},{6,4},{8,6},{10,8},{12,10},{14,12},{16,14},{18,... | collective-permute-start | bytes 2162696 | tf_op jit(solution)/shard_map/ppermute | solution.py:16
  223.0 111.9 %copy-start.4 = (bf16[2816,128]{1,0:T(8,128)(2,1)}, bf16[2816,128]{1,0:T(8,128)(2,1)S(1)}, u32[]{:S(2)}) copy-start(bf16[2816,128]{1,0:T(8,128)(2,1)S(1)} %collective-permute-done) | copy-start | bytes 2162692
  223.2 47.8 %collective-permute-start.1 = (bf16[2816,256]{1,0:T(8,128)(2,1)S(1)}, bf16[2816,256]{1,0:T(8,128)(2,1)S(1)}, u32[]{:S(2)}, u32[]{:S(2)}) collective-permute-start(bf16[2816,256]{1,0:T(8,128)(2,1)S(1)} %pad_maximum_fusion.2), channel_id=1, source_target_pairs={{0,28},{2,30},{4,0},{6,2},{8,4},{10,6},{12,8},{14,10},{16,12},{18,... | collective-permute-start | bytes 4325384 | tf_op jit(solution)/shard_map/ppermute | solution.py:16
  271.0 63.9 %copy-start = (bf16[2816,256]{1,0:T(8,128)(2,1)}, bf16[2816,256]{1,0:T(8,128)(2,1)S(1)}, u32[]{:S(2)}) copy-start(bf16[2816,256]{1,0:T(8,128)(2,1)S(1)} %collective-permute-done.1) | copy-start | bytes 4325380
  271.3 71.9 %copy-start.9 = (bf16[96,2048]{1,0:T(8,128)(2,1)S(1)}, bf16[96,2048]{1,0:T(8,128)(2,1)}, u32[]{:S(2)}) copy-start(bf16[96,2048]{1,0:T(8,128)(2,1)} %param.17) | copy-start | bytes 1179652
  271.3 71.9 %copy-start.11 = (f32[2048]{0:T(1024)S(1)}, f32[2048]{0:T(1024)}, u32[]{:S(2)}) copy-start(f32[2048]{0:T(1024)} %param.24) | copy-start | bytes 24580
  271.3 59.5 %collective-permute-start.2 = (bf16[2816,512]{1,0:T(8,128)(2,1)S(1)}, bf16[2816,512]{1,0:T(8,128)(2,1)S(1)}, u32[]{:S(2)}, u32[]{:S(2)}) collective-permute-start(bf16[2816,512]{1,0:T(8,128)(2,1)S(1)} %pad_maximum_fusion.1), channel_id=1, source_target_pairs={{0,24},{2,26},{4,28},{6,30},{8,0},{10,2},{12,4},{14,6},{16,8},{18,... | collective-permute-start | bytes 8650760 | tf_op jit(solution)/shard_map/ppermute | solution.py:16
  334.9 9.7 %copy-start.12 = (f32[2048]{0:T(1024)S(1)}, f32[2048]{0:T(1024)}, u32[]{:S(2)}) copy-start(f32[2048]{0:T(1024)} %param.25) | copy-start | bytes 24580
  334.9 356.3 %collective-permute-start.3 = (bf16[2816,1024]{1,0:T(8,128)(2,1)}, bf16[2816,1024]{1,0:T(8,128)(2,1)}, u32[]{:S(2)}, u32[]{:S(2)}) collective-permute-start(bf16[2816,1024]{1,0:T(8,128)(2,1)} %pad_maximum_fusion), channel_id=1, source_target_pairs={{0,16},{2,18},{4,20},{6,22},{8,24},{10,26},{12,28},{14,30},{16,0},... | collective-permute-start | bytes 17301512 | tf_op jit(solution)/shard_map/ppermute | solution.py:16
  350.4 346.5 %copy-start.3 = (bf16[2816,128]{1,0:T(8,128)(2,1)S(1)}, bf16[2816,128]{1,0:T(8,128)(2,1)}, u32[]{:S(2)}) copy-start(bf16[2816,128]{1,0:T(8,128)(2,1)} %param.29) | copy-start | bytes 2162692
  350.4 347.5 %copy-start.5 = (bf16[2816,128]{1,0:T(8,128)(2,1)S(1)}, bf16[2816,128]{1,0:T(8,128)(2,1)}, u32[]{:S(2)}) copy-start(bf16[2816,128]{1,0:T(8,128)(2,1)} %copy-done.4) | copy-start | bytes 2162692
  350.4 348.4 %copy-start.1 = (bf16[2816,256]{1,0:T(8,128)(2,1)S(1)}, bf16[2816,256]{1,0:T(8,128)(2,1)}, u32[]{:S(2)}) copy-start(bf16[2816,256]{1,0:T(8,128)(2,1)} %copy-done) | copy-start | bytes 4325380
  701.9 6.4 copy-start.10
  716.4 116.6 %copy-start.6 = (bf16[96,2048]{1,0:T(8,128)(2,1)S(1)}, bf16[96,2048]{1,0:T(8,128)(2,1)}, u32[]{:S(2)}) copy-start(bf16[96,2048]{1,0:T(8,128)(2,1)} %reduce-scatter.3.cloned.1.call-done) | copy-start | bytes 1179652
  716.4 116.6 %copy-start.13 = (f32[2048]{0:T(1024)S(1)}, f32[2048]{0:T(1024)}, u32[]{:S(2)}) copy-start(f32[2048]{0:T(1024)} %param.26) | copy-start | bytes 24580
Sparse Core Ops, SparseCore 0:
  10.1 60.8 all-gather.5
  73.8 56.6 all-gather.7
  157.0 54.7 reduce-scatter.2
  214.4 399.3 all-gather.9
  616.4 194.7 all-gather.11
  825.3 6.4 reduce-scatter.4
